TPU v7x, 32 devices: a whole 2x2x4 slice. The times are simulated.
32 devices in a mesh: ep: 16 (over z, x, core), tp: 2 (over y).
Axes of the slice: x: 2, y: 2, z: 4, core: 2. Of those that a mesh axis runs over, the one named last changes fastest.
Arguments:
- tokens: bfloat16 [256, 2048], P('ep', 'tp'), may hold values from -6 to 6
- state: bfloat16 [256, 32, 4096], P('ep', 'tp'), may hold values from -6 to 6
- mix_gain: float32 [2048], P('tp'), may hold values from 0.1 to 1.9
- w_recept: bfloat16 [2048, 2048], P('tp', 'ep'), may hold values from -0.125 to 0.125
- w_key: bfloat16 [2048, 2048], P('tp', 'ep'), may hold values from -0.125 to 0.125
- w_value: bfloat16 [2048, 2048], P('tp', 'ep'), may hold values from -0.125 to 0.125
- w_decay: bfloat16 [2048, 2048], P('tp', 'ep'), may hold values from -0.125 to 0.125
- w_rate: bfloat16 [2048, 2048], P('tp', 'ep'), may hold values from -0.125 to 0.125
- decay_base: float32 [2048], P('tp'), may hold values from -4 to 2
- rate_base: float32 [2048], P('tp'), may hold values from -2 to 2
- head_gain: float32 [2048], P('tp'), may hold values from 0.1 to 1.9
- w_out: bfloat16 [2048, 2048], P('tp', 'ep'), may hold values from -0.125 to 0.125
- moe_gain: float32 [2048], replicated, may hold values from 0.1 to 1.9
- routes: int32 [256, 6], P('ep'), may hold values from 0 to 15, all different within a row; in each aligned block of 16 rows (0 to 15, 16 to 31, ...) at most 12 rows name the same one
- route_weight: float32 [256, 6], P('ep'), may hold values from 0.1 to 1
- expert_gate: bfloat16 [16, 2048, 512], P('ep', None, 'tp'), may hold values from -0.125 to 0.125
- expert_up: bfloat16 [16, 2048, 512], P('ep', None, 'tp'), may hold values from -0.125 to 0.125
- expert_down: bfloat16 [16, 512, 2048], P('ep', 'tp'), may hold values from -0.25 to 0.25
- shared_gate: bfloat16 [2048, 512], P(None, 'tp'), may hold values from -0.125 to 0.125
- shared_up: bfloat16 [2048, 512], P(None, 'tp'), may hold values from -0.125 to 0.125
- shared_down: bfloat16 [512, 2048], P('tp'), may hold values from -0.25 to 0.25
Outputs:
- layer_out: bfloat16 [256, 2048], P('ep', 'tp')
Inputs may be any that keep to these rules, and one draw needn't show every extreme that they name: `routes`: each row names 6 different experts. Within the rows of one device (aligned blocks of 16 rows) no expert is named by more than 12 rows, a bound that some block reaches.
All inputs are finite; a program needn't handle non-finite values.
Results may differ from a plain program's by a relative error of at most 0.024.
Values may be sent and summed in bfloat16 or wider, within the bound.
A program may use at most 64 MiB of HBM per device.

v0:
```python
import functools
import math

import jax
import jax.numpy as jnp
from jax import lax
from jax.experimental import pallas as pl
from jax.experimental.pallas import tpu as pltpu
from jax.sharding import PartitionSpec as P

HEAD = 64


RMS_EPS = 1e-06
GN_EPS = 0.00064
KEY_EPS = 1e-06
ROUTED_SCALE = 2.5
EXP_HALF = math.exp(-0.5)


def for_sending(array):
    return jax.tree.map(lambda a: a.astype(jnp.bfloat16) if a.dtype == jnp.float32 else a, array)


def mixer_rows(state_rows, projected, decay_base, rate_base, head_gain):
    seq_count = projected.shape[0]
    head_count = projected.shape[2] // HEAD

    def per_head(column):
        return projected[:, column, :].reshape(seq_count, head_count, HEAD)

    receptance = per_head(0)
    key_vec = per_head(1)
    value_vec = per_head(2)
    decay_pre = (projected[:, 3, :] + decay_base).reshape(seq_count, head_count, HEAD)
    rate_pre = (projected[:, 4, :] + rate_base).reshape(seq_count, head_count, HEAD)
    decay_rate = jnp.exp(-jnp.exp(-jax.nn.softplus(-decay_pre) - 0.5))
    in_rate = jax.nn.sigmoid(rate_pre)
    unit_key = key_vec * lax.rsqrt(jnp.sum(key_vec * key_vec, axis=-1, keepdims=True) + KEY_EPS)
    carried = state_rows.astype(jnp.float32).reshape(seq_count, head_count, HEAD, HEAD)
    removed = jnp.einsum("nhvk,nhk->nhv", carried, unit_key)
    updated = (
        carried * decay_rate[:, :, None, :]
        - removed[:, :, :, None] * (unit_key * in_rate)[:, :, None, :]
        + value_vec[:, :, :, None] * (key_vec * in_rate)[:, :, None, :]
    )
    readout = jnp.einsum("nhvk,nhk->nhv", updated, receptance)
    centre = jnp.mean(readout, axis=-1, keepdims=True)
    spread = jnp.mean(jnp.square(readout - centre), axis=-1, keepdims=True)
    normed = (readout - centre) * lax.rsqrt(spread + GN_EPS)
    return (normed.reshape(seq_count, head_count * HEAD) * head_gain).astype(jnp.bfloat16)


def quarter_sums(partial_value):
    return jax.tree.map(
        lambda part: part.astype(jnp.float32),
        lax.psum_scatter(for_sending(partial_value), "tp", scatter_dimension=2, tiled=True),
    )


def project_split(part_rows, weight_cols):
    inner_len = weight_cols.shape[0]
    role_count = weight_cols.shape[1]
    col_width = weight_cols.shape[2]
    flat_weight = weight_cols.reshape(inner_len, role_count * col_width)
    block_rows = lax.all_gather(part_rows, "ep", axis=0, tiled=True)
    product = jnp.dot(block_rows, flat_weight, preferred_element_type=jnp.float32)
    gathered = product.astype(jnp.bfloat16).reshape(block_rows.shape[0], role_count, col_width)
    owned = lax.all_to_all(gathered, "ep", split_axis=0, concat_axis=2, tiled=True)
    return quarter_sums(owned.astype(jnp.float32))


def body(
    tokens,
    state,
    mix_gain,
    w_recept,
    w_key,
    w_value,
    w_decay,
    w_rate,
    decay_base,
    rate_base,
    head_gain,
    w_out,
    moe_gain,
    routes,
    route_weight,
    expert_gate,
    expert_up,
    expert_down,
    shared_gate,
    shared_up,
    shared_down,
):
    seq_count = tokens.shape[0]
    quarter = tokens.shape[1]
    width_all = quarter * lax.axis_size("tp")
    ep_count = lax.axis_size("ep")
    topk_count = routes.shape[1]
    capacity = min(seq_count, max(2, 2 * seq_count * topk_count // ep_count))
    tokens32 = tokens.astype(jnp.float32)
    square_sum = lax.psum(jnp.sum(tokens32 * tokens32, axis=1), "tp")
    factor = lax.rsqrt(square_sum / width_all + RMS_EPS)
    normed = (tokens32 * factor[:, None] * mix_gain).astype(jnp.bfloat16)
    stacked = jnp.stack((w_recept, w_key, w_value, w_decay, w_rate), axis=1)
    projected = project_split(normed, stacked)
    mixed = mixer_rows(state, projected, decay_base, rate_base, head_gain)
    attended = project_split(mixed, w_out[:, None, :])[:, 0, :]
    resid = (tokens32 + attended).astype(jnp.bfloat16)
    full_resid = lax.all_gather(resid, "tp", axis=1, tiled=True).astype(jnp.float32)
    moe_factor = lax.rsqrt(jnp.mean(full_resid * full_resid, axis=1, keepdims=True) + RMS_EPS)
    normed_two = (full_resid * moe_factor * moe_gain).astype(jnp.bfloat16)
    shared_hidden = (
        jax.nn.silu(jnp.dot(normed_two, shared_gate, preferred_element_type=jnp.float32))
        * jnp.dot(normed_two, shared_up, preferred_element_type=jnp.float32)
    ).astype(jnp.bfloat16)
    shared_part = jnp.dot(shared_hidden, shared_down, preferred_element_type=jnp.float32)
    entry_count = seq_count * topk_count
    flat_routes = routes.reshape(entry_count)
    position = jnp.arange(entry_count, dtype=jnp.int32)
    earlier = (flat_routes[:, None] == flat_routes[None, :]) & (
        position[None, :] < position[:, None]
    )
    rank_in = jnp.sum(earlier.astype(jnp.int32), axis=1)
    local_slot = flat_routes * capacity + rank_in
    slot_count = ep_count * capacity
    slot_ids = jnp.arange(slot_count, dtype=jnp.int32)
    matches = (slot_ids[:, None] == local_slot[None, :]).astype(jnp.float32)
    dispatch_map = jnp.sum(matches.reshape(slot_count, seq_count, topk_count), axis=2).astype(
        jnp.bfloat16
    )
    outgoing = jnp.dot(dispatch_map, normed_two, preferred_element_type=jnp.float32)
    outgoing = outgoing.astype(jnp.bfloat16).reshape(ep_count, capacity, width_all)
    arrived = lax.all_to_all(outgoing, "ep", split_axis=0, concat_axis=0, tiled=True)
    expert_in = arrived.reshape(slot_count, width_all)
    hidden = (
        jax.nn.silu(jnp.dot(expert_in, expert_gate[0], preferred_element_type=jnp.float32))
        * jnp.dot(expert_in, expert_up[0], preferred_element_type=jnp.float32)
    ).astype(jnp.bfloat16)
    expert_part = jnp.dot(hidden, expert_down[0], preferred_element_type=jnp.float32)
    routed_sum, shared_sum = quarter_sums((expert_part[:, None, :], shared_part[:, None, :]))
    expert_out = routed_sum[:, 0, :].astype(jnp.bfloat16).reshape(ep_count, capacity, quarter)
    came_back = lax.all_to_all(expert_out, "ep", split_axis=0, concat_axis=0, tiled=True).reshape(
        slot_count, quarter
    )
    picked = (
        jnp.take(came_back, local_slot, axis=0)
        .astype(jnp.float32)
        .reshape(seq_count, topk_count, quarter)
    )
    share = route_weight / jnp.sum(route_weight, axis=1, keepdims=True) * ROUTED_SCALE
    routed = jnp.sum(share[:, :, None] * picked, axis=1)
    return (resid.astype(jnp.float32) + routed + shared_sum[:, 0, :]).astype(jnp.bfloat16)


def fits_fused(ep_count, tp_count, col_width, head_rows, quarter):
    return (
        tp_count > 1
        and ep_count % (2 * tp_count) == 0
        and ep_count >= 8
        and ep_count & (ep_count - 1) == 0
        and ep_count <= HEAD
        and col_width % 128 == 0
        and quarter % 128 == 0
        and head_rows % 16 == 0
    )


def fused_kernel(
    dims,
    tokens,
    state,
    mix_gain,
    w_recept,
    w_key,
    w_value,
    w_decay,
    w_rate,
    decay_base,
    rate_base,
    head_gain,
    w_out,
    moe_gain,
    routes,
    route_weight,
    expert_gate,
    expert_up,
    expert_down,
    shared_gate,
    shared_up,
    shared_down,
    out,
    tok_buf,
    tok_full,
    prod_buf,
    prod_in,
    mix_buf,
    att_buf,
    att_in,
    norm_buf,
    y_buf,
    y_in,
    x_buf,
    x_in,
    z_buf,
    z_in,
    head_buf,
    ones_map,
    v_state,
    v_w,
    v_wout,
    v_gate,
    v_up,
    v_down,
    v_sgate,
    v_sup,
    v_sdown,
    load_sem,
    tok_send,
    tok_recv,
    tp_send,
    tp_recv,
    prod_send,
    prod_recv,
    mix_send,
    mix_recv,
    att_send,
    att_recv,
    norm_send,
    norm_recv,
    sis_send,
    sis_recv,
    x_send,
    x_recv,
    z_send,
    z_recv,
):
    ep_n, tp_n, seq, quarter, colw, width = dims
    f32, bf16 = jnp.float32, jnp.bfloat16
    chips = ep_n // 2
    group = ep_n // tp_n
    heads = quarter // HEAD
    rows = seq * heads
    pair_cols = colw // 128
    me = lax.axis_index("ep")
    my_t = lax.axis_index("tp")
    core = lax.rem(me, 2)
    chip = me // 2
    sister = chip * 2 + 1 - core
    planes = chips // 2
    plane, side = chip // 2, lax.rem(chip, 2)
    across = (plane * 2 + 1 - side) * 2 + core

    def remote(src, dst, send, recv, ep_to, tp_to):
        return pltpu.make_async_remote_copy(
            src_ref=src,
            dst_ref=dst,
            send_sem=send,
            recv_sem=recv,
            device_id={"ep": ep_to, "tp": tp_to},
            device_id_type=pl.DeviceIdType.MESH,
        )

    loads = []

    def load(src, dst):
        copy = pltpu.make_async_copy(src, dst, load_sem.at[len(loads)])
        copy.start()
        loads.append(copy)
        return copy

    ld_tok = load(tokens, tok_buf.at[me])
    ld_tokf = load(tokens, tok_full.at[my_t])
    ld_w = [
        load(w, v_w.at[:, pl.ds(p * colw, colw)])
        for p, w in enumerate((w_recept, w_key, w_value, w_decay, w_rate))
    ]
    ld_state = load(state, v_state)
    ld_wout = load(w_out, v_wout)
    ld_sg = load(shared_gate, v_sgate)
    ld_su = load(shared_up, v_sup)
    ld_sd = load(shared_down, v_sdown)
    ld_eg = load(expert_gate, v_gate)
    ld_eu = load(expert_up, v_up)
    ld_ed = load(expert_down, v_down)

    barrier = pltpu.get_barrier_semaphore()

    def greet(k, carry):
        e_to = lax.rem(me + k // tp_n, ep_n)
        t_to = lax.rem(my_t + lax.rem(k, tp_n), tp_n)
        pl.semaphore_signal(
            barrier,
            inc=1,
            device_id={"ep": e_to, "tp": t_to},
            device_id_type=pl.DeviceIdType.MESH,
        )
        return carry

    lax.fori_loop(1, ep_n * tp_n, greet, 0)

    big_rows = ones_map.shape[0]
    row_id = lax.broadcasted_iota(jnp.int32, (big_rows, 128), 0)
    lane_id = lax.broadcasted_iota(jnp.int32, (big_rows, 128), 1)
    ones_map[...] = jnp.where(row_id // HEAD == lane_id % HEAD, 1.0, 0.0).astype(bf16)

    ld_tok.wait()
    pl.semaphore_wait(barrier, ep_n * tp_n - 1)

    def gather_start(buf, send, recv):
        remote(buf.at[me], buf.at[me], send.at[0], recv.at[me], sister, my_t).start()

        def go(k, carry):
            to = lax.rem(chip + k, chips) * 2 + core
            remote(buf.at[me], buf.at[me], send.at[k], recv.at[me], to, my_t).start()
            return carry

        lax.fori_loop(1, chips, go, 0)

    def gather_finish(buf, send, recv):
        def forward(k, carry):
            src = lax.rem(chip + chips - k, chips) * 2 + core
            remote(buf.at[src], buf.at[src], send.at[0], recv.at[src], sister, my_t).wait_recv()
            remote(
                buf.at[src], buf.at[src], send.at[chips + k], recv.at[src], sister, my_t
            ).start()
            return carry

        lax.fori_loop(1, chips, forward, 0)

        def finish(k, carry):
            src = lax.rem(chip + chips - k, chips) * 2 + 1 - core
            remote(buf.at[src], buf.at[src], send.at[0], recv.at[src], sister, my_t).wait_recv()
            return carry

        lax.fori_loop(0, chips, finish, 0)

    def flip(z, k):
        bit = 1
        res = z
        while bit <= k:
            if k & bit:
                res = res + bit * (1 - 2 * lax.rem(z // bit, 2))
            bit *= 2
        return res

    def plane_gather_start(buf, send, recv):
        def put(i, to):
            remote(buf.at[me], buf.at[me], send.at[i], recv.at[me], to, my_t).start()

        for k in range(planes - 1, 0, -1):
            put(k, (flip(plane, k) * 2 + side) * 2 + core)
        put(planes, across)
        put(0, sister)

    def plane_gather_finish(buf, send, recv):
        def arrived(src):
            remote(buf.at[src], buf.at[src], send.at[0], recv.at[src], me, my_t).wait_recv()

        def forward(i, src, to):
            remote(buf.at[src], buf.at[src], send.at[i], recv.at[src], to, my_t).start()

        arrived(across)
        forward(3 * planes - 1, across, sister)
        for k in range(planes - 1, 0, -1):
            src = (flip(plane, k) * 2 + side) * 2 + core
            arrived(src)
            forward(planes + k, src, across)
            forward(2 * planes - 1 + k, src, sister)
        for k in range(planes - 1, 0, -1):
            src = (flip(plane, k) * 2 + 1 - side) * 2 + core
            arrived(src)
            forward(3 * planes - 1 + k, src, sister)

        def finish(k, carry):
            arrived(lax.rem(chip + k, chips) * 2 + 1 - core)
            return carry

        lax.fori_loop(0, chips, finish, 0)

    def plane_gather_drain(buf, send, recv):
        def drain(k, carry):
            remote(buf.at[me], buf.at[me], send.at[k], recv.at[me], sister, my_t).wait_send()
            return carry

        lax.fori_loop(0, 4 * planes - 1, drain, 0)

    def gather_drain(buf, send, recv):
        def drain(k, carry):
            remote(buf.at[me], buf.at[me], send.at[k], recv.at[me], sister, my_t).wait_send()
            return carry

        lax.fori_loop(0, chips, drain, 0)
        lax.fori_loop(chips + 1, 2 * chips, drain, 0)

    gather_start(tok_buf, tok_send, tok_recv)
    for j in range(1, tp_n):
        remote(
            tok_buf.at[me],
            tok_full.at[my_t],
            tp_send.at[j],
            tp_recv.at[my_t],
            me,
            lax.rem(my_t + j, tp_n),
        ).start()

    weight = route_weight[...]
    share = weight / jnp.sum(weight, axis=0, keepdims=True) * ROUTED_SCALE
    experts = lax.broadcasted_iota(jnp.int32, (128, seq), 0) % HEAD
    dense = jnp.zeros((128, seq), f32)
    for k in range(routes.shape[0]):
        dense += jnp.where(routes[k : k + 1, :] == experts, share[k : k + 1, :], 0.0)
    dense = dense.T
    lanes = lax.broadcasted_iota(jnp.int32, (seq, 128), 1)
    high = dense.astype(bf16).astype(f32)
    norm_buf[me, :, width:] = jnp.where(lanes < HEAD, high, dense - high).astype(bf16)

    for copy in ld_w:
        copy.wait()
    gather_finish(tok_buf, tok_send, tok_recv)
    scaled = (tok_buf[...].astype(f32).reshape(ep_n * seq, quarter) * mix_gain[...]).astype(bf16)
    product = jnp.dot(scaled, v_w[...], preferred_element_type=f32)
    prod_buf[...] = product.astype(bf16).reshape(ep_n, seq, 5 * colw)

    owner = me // group
    slot = lax.rem(me, group)

    @pl.when(owner == my_t)
    def _():
        prod_in[my_t, slot] = prod_buf[me]

    @pl.when(owner != my_t)
    def _():
        remote(
            prod_buf.at[me], prod_in.at[my_t, slot], prod_send.at[0], prod_recv.at[my_t, slot], me, owner
        ).start()

    def send_prod(k, carry):
        to = lax.rem(me + k, ep_n)
        remote(
            prod_buf.at[to], prod_in.at[my_t, slot], prod_send.at[k], prod_recv.at[my_t, slot], to, owner
        ).start()
        return carry

    lax.fori_loop(1, ep_n, send_prod, 0)
    gather_drain(tok_buf, tok_send, tok_recv)

    ld_tokf.wait()
    for j in range(1, tp_n):
        src = lax.rem(my_t + j, tp_n)
        remote(
            tok_buf.at[me], tok_full.at[src], tp_send.at[j], tp_recv.at[src], me, src
        ).wait_recv()
    square_sum = jnp.zeros((seq, 1), f32)
    for t in range(tp_n):
        part = tok_full[t].astype(f32)
        square_sum += jnp.sum(part * part, axis=1, keepdims=True)
    factor = lax.rsqrt(square_sum / width + RMS_EPS)
    ld_state.wait()

    def recv_prod(k, carry):
        src_t, src_slot = k // group, lax.rem(k, group)
        mine = (src_t == my_t) & (my_t * group + src_slot == me)

        @pl.when(jnp.logical_not(mine))
        def _():
            remote(
                prod_buf.at[0],
                prod_in.at[src_t, src_slot],
                prod_send.at[0],
                prod_recv.at[src_t, src_slot],
                me,
                my_t,
            ).wait_recv()

        return carry

    lax.fori_loop(0, tp_n * group, recv_prod, 0)

    low_half = lax.broadcasted_iota(jnp.int32, (seq, 128), 1) < HEAD
    for g in range(group):
        total = prod_in[0, g].astype(f32)
        for t in range(1, tp_n):
            total += prod_in[t, g].astype(f32)
        total = total * factor
        for p in range(5):
            for i in range(pair_cols):
                pair = g * pair_cols + i
                val = total[:, p * colw + i * 128 : p * colw + (i + 1) * 128]
                if p == 3:
                    val = val + decay_base[:, pair * 128 : (pair + 1) * 128]
                if p == 4:
                    val = val + rate_base[:, pair * 128 : (pair + 1) * 128]
                turned = pltpu.roll(val, HEAD, 1)
                head_buf[p, pl.ds(2 * pair, seq, stride=heads), :] = jnp.where(low_half, val, turned)
                head_buf[p, pl.ds(2 * pair + 1, seq, stride=heads), :] = jnp.where(
                    low_half, turned, val
                )

    def half_sum(x):
        return 0.5 * jnp.sum(x, axis=1, keepdims=True)

    recept, key, value = head_buf[0], head_buf[1], head_buf[2]
    decay = jnp.exp(-jax.nn.sigmoid(head_buf[3]) * EXP_HALF)
    rate = jax.nn.sigmoid(head_buf[4])
    unit = key * lax.rsqrt(half_sum(key * key) + KEY_EPS)
    rated = rate * recept
    removed_by = half_sum(unit * rated)
    added_by = half_sum(key * rated)
    left = (decay * recept).astype(bf16)
    right = unit.astype(bf16)
    step = 512
    left_wide = jnp.concatenate([left] * (step // 128), axis=1)
    right_wide = jnp.concatenate([right] * (step // 128), axis=1)
    read_left = jnp.zeros((rows, 128), f32)
    read_right = jnp.zeros((rows, 128), f32)
    for c in range(HEAD * HEAD // step):
        block = v_state[:, c * step : (c + 1) * step]
        ones = ones_map[c * step : (c + 1) * step, :]
        read_left += jnp.dot(block * left_wide, ones, preferred_element_type=f32)
        read_right += jnp.dot(block * right_wide, ones, preferred_element_type=f32)
    readout = read_left - read_right * removed_by + value * added_by
    centred = readout - half_sum(readout) / HEAD
    spread = half_sum(centred * centred) / HEAD
    head_buf[0] = centred * lax.rsqrt(spread + GN_EPS)
    for pair in range(heads // 2):
        even = head_buf[0, pl.ds(2 * pair, seq, stride=heads), :]
        odd = head_buf[0, pl.ds(2 * pair + 1, seq, stride=heads), :]
        cols = slice(pair * 128, (pair + 1) * 128)
        mix_buf[me, :, cols] = (jnp.where(low_half, even, odd) * head_gain[:, cols]).astype(bf16)

    gather_start(mix_buf, mix_send, mix_recv)

    @pl.when(owner != my_t)
    def _():
        remote(
            prod_buf.at[me], prod_in.at[my_t, slot], prod_send.at[0], prod_recv.at[my_t, slot], me, owner
        ).wait_send()

    def drain_prod(k, carry):
        remote(
            prod_buf.at[me], prod_in.at[my_t, slot], prod_send.at[k], prod_recv.at[my_t, slot], me, owner
        ).wait_send()
        return carry

    lax.fori_loop(1, ep_n, drain_prod, 0)
    for j in range(1, tp_n):
        remote(
            tok_buf.at[me], tok_full.at[my_t], tp_send.at[j], tp_recv.at[my_t], me, my_t
        ).wait_send()
    ld_wout.wait()
    gather_finish(mix_buf, mix_send, mix_recv)
    product = jnp.dot(
        mix_buf[...].reshape(ep_n * seq, quarter), v_wout[...], preferred_element_type=f32
    )
    att_buf[...] = product.astype(bf16).reshape(ep_n, seq, colw)
    att_in[my_t, me] = att_buf[me]

    def send_att(k, carry):
        e_to = lax.rem(me + k // tp_n, ep_n)
        t_to = lax.rem(my_t + lax.rem(k, tp_n), tp_n)
        remote(
            att_buf.at[e_to], att_in.at[my_t, me], att_send.at[k], att_recv.at[my_t, me], e_to, t_to
        ).start()
        return carry

    lax.fori_loop(1, ep_n * tp_n, send_att, 0)
    gather_drain(mix_buf, mix_send, mix_recv)

    def recv_att(k, carry):
        e_from = lax.rem(me + k // tp_n, ep_n)
        t_from = lax.rem(my_t + lax.rem(k, tp_n), tp_n)
        remote(
            att_buf.at[0], att_in.at[t_from, e_from], att_send.at[k], att_recv.at[t_from, e_from], me, my_t
        ).wait_recv()
        return carry

    lax.fori_loop(1, ep_n * tp_n, recv_att, 0)
    square_sum = jnp.zeros((seq, 1), f32)
    parts = []
    for e in range(ep_n):
        attended = att_in[0, e].astype(f32)
        for t in range(1, tp_n):
            attended += att_in[t, e].astype(f32)
        col = e * colw
        token = tok_full[col // quarter, :, col % quarter : col % quarter + colw].astype(f32)
        part = (token + attended).astype(bf16).astype(f32)
        parts.append(part)
        square_sum += jnp.sum(part * part, axis=1, keepdims=True)
    factor = lax.rsqrt(square_sum / width + RMS_EPS)
    for e in range(ep_n):
        cols = slice(e * colw, (e + 1) * colw)
        norm_buf[me, :, cols] = (parts[e] * factor * moe_gain[:, cols]).astype(bf16)

    plane_gather_start(norm_buf, norm_send, norm_recv)

    def drain_att(k, carry):
        remote(
            att_buf.at[me], att_in.at[my_t, me], att_send.at[k], att_recv.at[my_t, me], me, my_t
        ).wait_send()
        return carry

    lax.fori_loop(1, ep_n * tp_n, drain_att, 0)

    def gated(x, gate, up):
        g = jnp.dot(x, gate, preferred_element_type=f32)
        u = jnp.dot(x, up, preferred_element_type=f32)
        return (g * jax.nn.sigmoid(g) * u).astype(bf16)

    for copy in (ld_sg, ld_su, ld_sd):
        copy.wait()
    own = norm_buf[me, :, :width]
    shared_hidden = gated(own, v_sgate[...], v_sup[...])
    shared_part = jnp.dot(shared_hidden, v_sdown[...], preferred_element_type=f32)
    for copy in (ld_eg, ld_eu, ld_ed):
        copy.wait()
    plane_gather_finish(norm_buf, norm_send, norm_recv)
    hidden = gated(norm_buf[:, :, :width].reshape(ep_n * seq, width), v_gate[0], v_up[0])
    tail = norm_buf[:, :, width:].astype(f32).reshape(ep_n * seq, 128)
    lanes = lax.broadcasted_iota(jnp.int32, (ep_n * seq, 128), 1)
    mine = jnp.sum(jnp.where(lanes % HEAD == me, tail, 0.0), axis=1, keepdims=True)
    routed = jnp.dot(hidden, v_down[0], preferred_element_type=f32) * mine
    routed = routed.reshape(chips, 2, seq, width)
    for c in range(2):
        y_buf[c] = routed[:, c].astype(bf16)
    y_buf[core, chip] = (y_buf[core, chip].astype(f32) + shared_part).astype(bf16)
    order = list(range(planes - 1, -1, -1))

    def to_sister(c):
        return remote(
            y_buf.at[1 - core, c], y_in.at[c], sis_send.at[c], sis_recv.at[c], sister, my_t
        )

    def to_across(z):
        return remote(x_buf.at[z], x_in.at[z], x_send.at[z], x_recv.at[z], across, my_t)

    for k in order:
        to_sister(flip(plane, k) * 2 + 1 - side).start()
    for k in order:
        to_sister(flip(plane, k) * 2 + side).start()
    for k in order:
        z = flip(plane, k)
        c = z * 2 + 1 - side
        to_sister(c).wait_recv()
        x_buf[z] = (y_buf[core, c].astype(f32) + y_in[c].astype(f32)).astype(bf16)
        to_across(z).start()
    for k in order:
        z = flip(plane, k)
        c = z * 2 + side
        to_sister(c).wait_recv()
        to_across(z).wait_recv()
        joined = y_buf[core, c].astype(f32) + y_in[c].astype(f32) + x_in[z].astype(f32)
        for t in range(tp_n):
            z_buf[t, z] = joined[:, t * quarter : (t + 1) * quarter].astype(bf16)
        for j in range(tp_n - 1, -1, -1):
            t_to = lax.rem(my_t + j, tp_n)
            if k == 0 and j == 0:
                z_in[my_t, plane] = z_buf[my_t, plane]
            else:
                remote(
                    z_buf.at[t_to, z],
                    z_in.at[my_t, plane],
                    z_send.at[k * tp_n + j],
                    z_recv.at[my_t, plane],
                    (z * 2 + side) * 2 + core,
                    t_to,
                ).start()
    plane_gather_drain(norm_buf, norm_send, norm_recv)

    def drain_steps(c, carry):
        to_sister(c).wait_send()
        return carry

    lax.fori_loop(0, chips, drain_steps, 0)

    def drain_across(z, carry):
        to_across(z).wait_send()
        return carry

    lax.fori_loop(0, planes, drain_across, 0)
    for k in order:
        for j in range(tp_n):
            if k or j:
                t_from = lax.rem(my_t + j, tp_n)
                z = flip(plane, k)
                remote(
                    z_buf.at[0, 0], z_in.at[t_from, z], z_send.at[0], z_recv.at[t_from, z], me, my_t
                ).wait_recv()
    total = jnp.zeros((seq, quarter), f32)
    for t in range(tp_n):
        for c in range(planes):
            total += z_in[t, c].astype(f32)
    for g in range(group):
        cols = slice(g * colw, (g + 1) * colw)
        e = my_t * group + g
        attended = att_in[0, e].astype(f32)
        for t in range(1, tp_n):
            attended += att_in[t, e].astype(f32)
        part = (tok_full[my_t, :, cols].astype(f32) + attended).astype(bf16).astype(f32)
        out[:, cols] = (part + total[:, cols]).astype(bf16)

    def drain_z(k, carry):
        remote(
            z_buf.at[0, 0], z_in.at[my_t, plane], z_send.at[k], z_recv.at[my_t, plane], me, my_t
        ).wait_send()
        return carry

    lax.fori_loop(1, planes * tp_n, drain_z, 0)


def fused_body(*args):
    args = list(args)
    tokens, state, w_recept = args[0], args[1], args[3]
    seq, quarter = tokens.shape
    ep_n, tp_n = lax.axis_size("ep"), lax.axis_size("tp")
    colw = w_recept.shape[1]
    width = quarter * tp_n
    heads = state.shape[1]
    chips, group = ep_n // 2, ep_n // tp_n
    args[1] = state.reshape(seq * heads, state.shape[2])
    for i in (2, 8, 9, 10, 12):
        args[i] = args[i].reshape(1, -1)
    for i in (13, 14):
        args[i] = args[i].T
    hidden, shared = args[15].shape[2], args[18].shape[1]
    bf16, dma = jnp.bfloat16, pltpu.SemaphoreType.DMA
    vmem = {2, 8, 9, 10, 12, 13, 14}
    specs = [
        pl.BlockSpec(memory_space=pltpu.VMEM if i in vmem else pl.ANY) for i in range(len(args))
    ]
    scratch = [
        pltpu.VMEM((ep_n, seq, quarter), bf16),
        pltpu.VMEM((tp_n, seq, quarter), bf16),
        pltpu.VMEM((ep_n, seq, 5 * colw), bf16),
        pltpu.VMEM((tp_n, group, seq, 5 * colw), bf16),
        pltpu.VMEM((ep_n, seq, quarter), bf16),
        pltpu.VMEM((ep_n, seq, colw), bf16),
        pltpu.VMEM((tp_n, ep_n, seq, colw), bf16),
        pltpu.VMEM((ep_n, seq, width + 128), bf16),
        pltpu.VMEM((2, chips, seq, width), bf16),
        pltpu.VMEM((chips, seq, width), bf16),
        pltpu.VMEM((chips // 2, seq, width), bf16),
        pltpu.VMEM((chips // 2, seq, width), bf16),
        pltpu.VMEM((tp_n, chips // 2, seq, quarter), bf16),
        pltpu.VMEM((tp_n, chips // 2, seq, quarter), bf16),
        pltpu.VMEM((5, seq * heads, 128), jnp.float32),
        pltpu.VMEM((HEAD * HEAD, 128), bf16),
        pltpu.VMEM(args[1].shape, bf16),
        pltpu.VMEM((quarter, 5 * colw), bf16),
        pltpu.VMEM((quarter, colw), bf16),
        pltpu.VMEM((1, width, hidden), bf16),
        pltpu.VMEM((1, width, hidden), bf16),
        pltpu.VMEM((1, hidden, width), bf16),
        pltpu.VMEM((width, shared), bf16),
        pltpu.VMEM((width, shared), bf16),
        pltpu.VMEM((shared, width), bf16),
        dma((16,)),
        dma((ep_n,)),
        dma((ep_n,)),
        dma((tp_n,)),
        dma((tp_n,)),
        dma((ep_n,)),
        dma((tp_n, group)),
        dma((ep_n,)),
        dma((ep_n,)),
        dma((ep_n * tp_n,)),
        dma((tp_n, ep_n)),
        dma((ep_n,)),
        dma((ep_n,)),
        dma((chips,)),
        dma((chips,)),
        dma((chips // 2,)),
        dma((chips // 2,)),
        dma((chips // 2 * tp_n,)),
        dma((tp_n, chips // 2)),
    ]
    return pl.pallas_call(
        functools.partial(fused_kernel, (ep_n, tp_n, seq, quarter, colw, width)),
        out_shape=jax.ShapeDtypeStruct((seq, quarter), bf16),
        in_specs=specs,
        out_specs=pl.BlockSpec(memory_space=pltpu.VMEM),
        scratch_shapes=scratch,
        compiler_params=pltpu.CompilerParams(
            collective_id=0, has_side_effects=True, vmem_limit_bytes=60 * 1024 * 1024
        ),
        name="layer_step",
    )(*args)


def layer(*args):
    ep_n, tp_n = lax.axis_size("ep"), lax.axis_size("tp")
    if fits_fused(ep_n, tp_n, args[3].shape[1], args[1].shape[1], args[0].shape[1]):
        return fused_body(*args)
    return body(*args)


def solution(mesh):
    placed = (
        P("ep", "tp"),
        P("ep", "tp", None),
        P("tp"),
        P("tp", "ep"),
        P("tp", "ep"),
        P("tp", "ep"),
        P("tp", "ep"),
        P("tp", "ep"),
        P("tp"),
        P("tp"),
        P("tp"),
        P("tp", "ep"),
        P(),
        P("ep", None),
        P("ep", None),
        P("ep", None, "tp"),
        P("ep", None, "tp"),
        P("ep", "tp", None),
        P(None, "tp"),
        P(None, "tp"),
        P("tp", None),
    )
    return jax.shard_map(layer, mesh=mesh, in_specs=placed, out_specs=P("ep", "tp"), check_vma=False)
```

profile of v0, /device:TPU:0, one launch (start us, length us, event | category | flops | bytes accessed | tf_op | source)
XLA Modules:
  0.0 70.9 jit_solution(15825440269723130956)
XLA Ops:
  0.0 69.5 %layer_step.1 = bf16[16,1024]{1,0:T(8,128)(2,1)} custom-call(bf16[16,1024]{1,0:T(8,128)(2,1)} %tokens.1, bf16[256,4096]{1,0:T(8,128)(2,1)} %bitcast.8, f32[1,1024]{1,0:T(1,128)} %bitcast.10, bf16[1024,128]{1,0:T(8,128)(2,1)} %w_recept.1, bf16[1024,128]{1,0:T(8,128)(2,1)} %w_key.1, bf16[1024,128]{1,0:T(8,128)(2,1)} %w_value.1, bf16[1024,128]{1,0:T(8,128)(2,1)} %w_decay.1, ...), custom_call_target="tpu_custom_call" | custom-call | tf_op jit(solution)/shard_map/layer_step/pallas_call | solution.py:778
  69.5 1.4 %copy.23 = bf16[16,1024]{1,0:T(8,128)(2,1)} copy(bf16[16,1024]{1,0:T(8,128)(2,1)} %layer_step.1) | data formatting | bytes 65536
where the time goes:
time: 71.1 us; the launch traced here: 70.9 us
  Pallas kernels  69.5 us (98%)
  local copies, waits for them, and re-layouts  1.38 us (2%)
    pallas_call x1, Pallas kernels, fused_body(): pl.pallas_call(functools.partial(fused_kernel, (ep_n, tp_n, seq, quarter,...  69.5 us

commit v1 on v0

v1 whole, which is shorter than its diff:
```python
import functools
import math

import jax
import jax.numpy as jnp
from jax import lax
from jax.experimental import pallas as pl
from jax.experimental.pallas import tpu as pltpu
from jax.sharding import PartitionSpec as P

HEAD = 64


RMS_EPS = 1e-06
GN_EPS = 0.00064
KEY_EPS = 1e-06
ROUTED_SCALE = 2.5
EXP_HALF = math.exp(-0.5)


def for_sending(array):
    return jax.tree.map(lambda a: a.astype(jnp.bfloat16) if a.dtype == jnp.float32 else a, array)


def mixer_rows(state_rows, projected, decay_base, rate_base, head_gain):
    seq_count = projected.shape[0]
    head_count = projected.shape[2] // HEAD

    def per_head(column):
        return projected[:, column, :].reshape(seq_count, head_count, HEAD)

    receptance = per_head(0)
    key_vec = per_head(1)
    value_vec = per_head(2)
    decay_pre = (projected[:, 3, :] + decay_base).reshape(seq_count, head_count, HEAD)
    rate_pre = (projected[:, 4, :] + rate_base).reshape(seq_count, head_count, HEAD)
    decay_rate = jnp.exp(-jnp.exp(-jax.nn.softplus(-decay_pre) - 0.5))
    in_rate = jax.nn.sigmoid(rate_pre)
    unit_key = key_vec * lax.rsqrt(jnp.sum(key_vec * key_vec, axis=-1, keepdims=True) + KEY_EPS)
    carried = state_rows.astype(jnp.float32).reshape(seq_count, head_count, HEAD, HEAD)
    removed = jnp.einsum("nhvk,nhk->nhv", carried, unit_key)
    updated = (
        carried * decay_rate[:, :, None, :]
        - removed[:, :, :, None] * (unit_key * in_rate)[:, :, None, :]
        + value_vec[:, :, :, None] * (key_vec * in_rate)[:, :, None, :]
    )
    readout = jnp.einsum("nhvk,nhk->nhv", updated, receptance)
    centre = jnp.mean(readout, axis=-1, keepdims=True)
    spread = jnp.mean(jnp.square(readout - centre), axis=-1, keepdims=True)
    normed = (readout - centre) * lax.rsqrt(spread + GN_EPS)
    return (normed.reshape(seq_count, head_count * HEAD) * head_gain).astype(jnp.bfloat16)


def quarter_sums(partial_value):
    return jax.tree.map(
        lambda part: part.astype(jnp.float32),
        lax.psum_scatter(for_sending(partial_value), "tp", scatter_dimension=2, tiled=True),
    )


def project_split(part_rows, weight_cols):
    inner_len = weight_cols.shape[0]
    role_count = weight_cols.shape[1]
    col_width = weight_cols.shape[2]
    flat_weight = weight_cols.reshape(inner_len, role_count * col_width)
    block_rows = lax.all_gather(part_rows, "ep", axis=0, tiled=True)
    product = jnp.dot(block_rows, flat_weight, preferred_element_type=jnp.float32)
    gathered = product.astype(jnp.bfloat16).reshape(block_rows.shape[0], role_count, col_width)
    owned = lax.all_to_all(gathered, "ep", split_axis=0, concat_axis=2, tiled=True)
    return quarter_sums(owned.astype(jnp.float32))


def body(
    tokens,
    state,
    mix_gain,
    w_recept,
    w_key,
    w_value,
    w_decay,
    w_rate,
    decay_base,
    rate_base,
    head_gain,
    w_out,
    moe_gain,
    routes,
    route_weight,
    expert_gate,
    expert_up,
    expert_down,
    shared_gate,
    shared_up,
    shared_down,
):
    seq_count = tokens.shape[0]
    quarter = tokens.shape[1]
    width_all = quarter * lax.axis_size("tp")
    ep_count = lax.axis_size("ep")
    topk_count = routes.shape[1]
    capacity = min(seq_count, max(2, 2 * seq_count * topk_count // ep_count))
    tokens32 = tokens.astype(jnp.float32)
    square_sum = lax.psum(jnp.sum(tokens32 * tokens32, axis=1), "tp")
    factor = lax.rsqrt(square_sum / width_all + RMS_EPS)
    normed = (tokens32 * factor[:, None] * mix_gain).astype(jnp.bfloat16)
    stacked = jnp.stack((w_recept, w_key, w_value, w_decay, w_rate), axis=1)
    projected = project_split(normed, stacked)
    mixed = mixer_rows(state, projected, decay_base, rate_base, head_gain)
    attended = project_split(mixed, w_out[:, None, :])[:, 0, :]
    resid = (tokens32 + attended).astype(jnp.bfloat16)
    full_resid = lax.all_gather(resid, "tp", axis=1, tiled=True).astype(jnp.float32)
    moe_factor = lax.rsqrt(jnp.mean(full_resid * full_resid, axis=1, keepdims=True) + RMS_EPS)
    normed_two = (full_resid * moe_factor * moe_gain).astype(jnp.bfloat16)
    shared_hidden = (
        jax.nn.silu(jnp.dot(normed_two, shared_gate, preferred_element_type=jnp.float32))
        * jnp.dot(normed_two, shared_up, preferred_element_type=jnp.float32)
    ).astype(jnp.bfloat16)
    shared_part = jnp.dot(shared_hidden, shared_down, preferred_element_type=jnp.float32)
    entry_count = seq_count * topk_count
    flat_routes = routes.reshape(entry_count)
    position = jnp.arange(entry_count, dtype=jnp.int32)
    earlier = (flat_routes[:, None] == flat_routes[None, :]) & (
        position[None, :] < position[:, None]
    )
    rank_in = jnp.sum(earlier.astype(jnp.int32), axis=1)
    local_slot = flat_routes * capacity + rank_in
    slot_count = ep_count * capacity
    slot_ids = jnp.arange(slot_count, dtype=jnp.int32)
    matches = (slot_ids[:, None] == local_slot[None, :]).astype(jnp.float32)
    dispatch_map = jnp.sum(matches.reshape(slot_count, seq_count, topk_count), axis=2).astype(
        jnp.bfloat16
    )
    outgoing = jnp.dot(dispatch_map, normed_two, preferred_element_type=jnp.float32)
    outgoing = outgoing.astype(jnp.bfloat16).reshape(ep_count, capacity, width_all)
    arrived = lax.all_to_all(outgoing, "ep", split_axis=0, concat_axis=0, tiled=True)
    expert_in = arrived.reshape(slot_count, width_all)
    hidden = (
        jax.nn.silu(jnp.dot(expert_in, expert_gate[0], preferred_element_type=jnp.float32))
        * jnp.dot(expert_in, expert_up[0], preferred_element_type=jnp.float32)
    ).astype(jnp.bfloat16)
    expert_part = jnp.dot(hidden, expert_down[0], preferred_element_type=jnp.float32)
    routed_sum, shared_sum = quarter_sums((expert_part[:, None, :], shared_part[:, None, :]))
    expert_out = routed_sum[:, 0, :].astype(jnp.bfloat16).reshape(ep_count, capacity, quarter)
    came_back = lax.all_to_all(expert_out, "ep", split_axis=0, concat_axis=0, tiled=True).reshape(
        slot_count, quarter
    )
    picked = (
        jnp.take(came_back, local_slot, axis=0)
        .astype(jnp.float32)
        .reshape(seq_count, topk_count, quarter)
    )
    share = route_weight / jnp.sum(route_weight, axis=1, keepdims=True) * ROUTED_SCALE
    routed = jnp.sum(share[:, :, None] * picked, axis=1)
    return (resid.astype(jnp.float32) + routed + shared_sum[:, 0, :]).astype(jnp.bfloat16)


def fits_fused(ep_count, tp_count, col_width, head_rows, quarter):
    return (
        tp_count == 2
        and ep_count >= 8
        and ep_count & (ep_count - 1) == 0
        and ep_count <= HEAD
        and col_width % 128 == 0
        and quarter * tp_count == ep_count * col_width
        and head_rows % 16 == 0
    )


def fused_kernel(
    dims,
    tokens,
    state,
    mix_gain,
    w_recept,
    w_key,
    w_value,
    w_decay,
    w_rate,
    decay_base,
    rate_base,
    head_gain,
    w_out,
    moe_gain,
    routes,
    route_weight,
    expert_gate,
    expert_up,
    expert_down,
    shared_gate,
    shared_up,
    shared_down,
    out,
    tok_buf,
    sq_buf,
    prod_buf,
    prod_in,
    mix_buf,
    att_f,
    att_out,
    att_in,
    res_buf,
    y_buf,
    r_in,
    s_buf,
    z_in,
    head_buf,
    ones_map,
    v_state,
    v_w,
    v_wout,
    v_gate,
    v_up,
    v_down,
    v_sgate,
    v_sup,
    v_sdown,
    load_sem,
    swap_send,
    swap_recv,
    tok_send,
    tok_recv,
    sq_send,
    sq_recv,
    prod_send,
    prod_recv,
    mix_send,
    mix_recv,
    att_send,
    att_recv,
    res_send,
    res_recv,
    r_send,
    r_recv,
    s_send,
    s_recv,
):
    ep_n, tp_n, seq, quarter, colw, width = dims
    f32, bf16 = jnp.float32, jnp.bfloat16
    chips = ep_n // 2
    group = chips // tp_n
    planes = chips // 2
    cols = 2 * colw
    heads = quarter // HEAD
    rows = seq * heads
    pair_cols = cols // 128
    total_rows = chips * seq
    me = lax.axis_index("ep")
    my_t = lax.axis_index("tp")
    core = lax.rem(me, 2)
    chip = me // 2
    sister = chip * 2 + 1 - core
    plane, side = chip // 2, lax.rem(chip, 2)
    owner, slot = chip // group, lax.rem(chip, group)

    def remote(src, dst, send, recv, ep_to, tp_to):
        return pltpu.make_async_remote_copy(
            src_ref=src,
            dst_ref=dst,
            send_sem=send,
            recv_sem=recv,
            device_id={"ep": ep_to, "tp": tp_to},
            device_id_type=pl.DeviceIdType.MESH,
        )

    def at(z, x):
        return (z * 2 + x) * 2 + core

    def flip(z, k):
        bit = 1
        res = z
        while bit <= k:
            if k & bit:
                res = res + bit * (1 - 2 * lax.rem(z // bit, 2))
            bit *= 2
        return res

    loads = []

    def load(src, dst):
        copy = pltpu.make_async_copy(src, dst, load_sem.at[len(loads)])
        copy.start()
        loads.append(copy)
        return copy

    def w_slot(p):
        return v_w.at[:, pl.ds(pl.multiple_of(p * cols + core * colw, 128), colw)]

    own_expert = pl.ds(core, 1)
    w_list = (w_recept, w_key, w_value, w_decay, w_rate)
    wout_slot = v_wout.at[:, pl.ds(pl.multiple_of(core * colw, 128), colw)]
    ld_tok = load(tokens, tok_buf.at[chip, :, :quarter])
    ld_w = [load(w, w_slot(p)) for p, w in enumerate(w_list)]
    ld_state = load(state, v_state)
    ld_wout = load(w_out, wout_slot)
    ld_shared = [
        load(a, b) for a, b in ((shared_gate, v_sgate), (shared_up, v_sup), (shared_down, v_sdown))
    ]
    ld_expert = [
        load(a, b.at[own_expert])
        for a, b in ((expert_gate, v_gate), (expert_up, v_up), (expert_down, v_down))
    ]

    barrier = pltpu.get_barrier_semaphore()

    def greet_one(e_to, t_to):
        pl.semaphore_signal(
            barrier,
            inc=1,
            device_id={"ep": e_to, "tp": t_to},
            device_id_type=pl.DeviceIdType.MESH,
        )

    def greet(k, carry):
        greet_one(lax.rem(chip + k // tp_n, chips) * 2 + core, lax.rem(my_t + lax.rem(k, tp_n), tp_n))
        return carry

    lax.fori_loop(1, chips * tp_n, greet, 0)
    greet_one(sister, my_t)

    weight = route_weight[...]
    share = weight / jnp.sum(weight, axis=0, keepdims=True) * ROUTED_SCALE
    experts = lax.broadcasted_iota(jnp.int32, (128, seq), 0) % HEAD
    dense = jnp.zeros((128, seq), f32)
    for k in range(routes.shape[0]):
        dense += jnp.where(routes[k : k + 1, :] == experts, share[k : k + 1, :], 0.0)
    dense = dense.T
    lanes = lax.broadcasted_iota(jnp.int32, (seq, 128), 1)
    high = dense.astype(bf16).astype(f32)
    tok_buf[chip, :, quarter:] = jnp.where(lanes < HEAD, high, dense - high).astype(bf16)

    big_rows = ones_map.shape[0]
    row_id = lax.broadcasted_iota(jnp.int32, (big_rows, 128), 0)
    lane_id = lax.broadcasted_iota(jnp.int32, (big_rows, 128), 1)
    ones_map[...] = jnp.where(row_id // HEAD == lane_id % HEAD, 1.0, 0.0).astype(bf16)

    ld_tok.wait()
    own_tok = tok_buf[chip, :, :quarter].astype(f32)
    sq_buf[my_t] = jnp.broadcast_to(jnp.sum(own_tok * own_tok, axis=1, keepdims=True), (seq, 128))

    pl.semaphore_wait(barrier, chips * tp_n)

    far_first = list(range(planes - 1, 0, -1))

    def gather_start(buf, send, recv):
        def put(i, to):
            remote(buf.at[chip], buf.at[chip], send.at[i], recv.at[chip], to, my_t).start()

        for k in far_first:
            put(k, at(flip(plane, k), side))
        put(0, at(plane, 1 - side))

    def gather_finish(buf, send, recv):
        def arrived(src):
            remote(buf.at[src], buf.at[src], send.at[0], recv.at[src], me, my_t).wait_recv()

        for k in far_first:
            src = flip(plane, k) * 2 + side
            arrived(src)
            remote(
                buf.at[src], buf.at[src], send.at[planes - 1 + k], recv.at[src], at(plane, 1 - side), my_t
            ).start()
        for k in [0] + far_first:
            arrived(flip(plane, k) * 2 + 1 - side)

    def drain(count, make):
        def step(k, carry):
            make(k).wait_send()
            return carry

        lax.fori_loop(0, count, step, 0)

    def gather_drain(buf, send, recv):
        drain(
            2 * planes - 1,
            lambda k: remote(buf.at[chip], buf.at[chip], send.at[k], recv.at[chip], sister, my_t),
        )

    gather_start(tok_buf, tok_send, tok_recv)
    sq_copy = remote(sq_buf.at[my_t], sq_buf.at[my_t], sq_send, sq_recv, me, 1 - my_t)
    sq_copy.start()

    def swap(i, src, dst):
        return remote(src, dst, swap_send.at[i], swap_recv.at[i], sister, my_t)

    swap_w = [swap(p, w, w_slot(p)) for p, w in enumerate(w_list)]
    swap_late = [swap(5, w_out, wout_slot)] + [
        swap(6 + i, a, b.at[own_expert])
        for i, (a, b) in enumerate(((expert_gate, v_gate), (expert_up, v_up), (expert_down, v_down)))
    ]
    for copy in swap_w:
        copy.start()

    for copy in ld_w:
        copy.wait()
    for copy in swap_w:
        copy.wait_recv()
    gather_finish(tok_buf, tok_send, tok_recv)
    tok_all = tok_buf[:, :, :quarter].astype(f32).reshape(total_rows, quarter)
    scaled = (tok_all * mix_gain[...]).astype(bf16)
    product = jnp.dot(scaled, v_w[...], preferred_element_type=f32)
    prod_buf[...] = product.astype(bf16).reshape(chips, seq, 5 * cols)

    def prod_copy(k, to):
        return remote(
            prod_buf.at[to],
            prod_in.at[my_t, slot],
            prod_send.at[k],
            prod_recv.at[my_t, slot],
            to * 2 + core,
            owner,
        )

    for k in range(chips - 1, 0, -1):
        prod_copy(k, flip(chip, k)).start()

    @pl.when(owner == my_t)
    def _():
        prod_in[my_t, slot] = prod_buf[chip]

    @pl.when(owner != my_t)
    def _():
        prod_copy(0, chip).start()

    for copy in swap_late:
        copy.start()
    gather_drain(tok_buf, tok_send, tok_recv)
    for copy in swap_w:
        copy.wait_send()
    sq_copy.wait_send()
    remote(sq_buf.at[1 - my_t], sq_buf.at[1 - my_t], sq_send, sq_recv, me, my_t).wait_recv()
    factor = lax.rsqrt((sq_buf[0] + sq_buf[1])[:, :1] / width + RMS_EPS)
    ld_state.wait()

    def recv_prod(k, carry):
        src_t, src_slot = k // group, lax.rem(k, group)
        mine = (src_t == my_t) & (my_t * group + src_slot == chip)

        @pl.when(jnp.logical_not(mine))
        def _():
            remote(
                prod_buf.at[0],
                prod_in.at[src_t, src_slot],
                prod_send.at[0],
                prod_recv.at[src_t, src_slot],
                me,
                my_t,
            ).wait_recv()

        return carry

    lax.fori_loop(0, tp_n * group, recv_prod, 0)

    low_half = lax.broadcasted_iota(jnp.int32, (seq, 128), 1) < HEAD
    for g in range(group):
        total = prod_in[0, g].astype(f32)
        for t in range(1, tp_n):
            total += prod_in[t, g].astype(f32)
        total = total * factor
        for p in range(5):
            for i in range(pair_cols):
                pair = g * pair_cols + i
                val = total[:, p * cols + i * 128 : p * cols + (i + 1) * 128]
                if p == 3:
                    val = val + decay_base[:, pair * 128 : (pair + 1) * 128]
                if p == 4:
                    val = val + rate_base[:, pair * 128 : (pair + 1) * 128]
                turned = pltpu.roll(val, HEAD, 1)
                head_buf[p, pl.ds(2 * pair, seq, stride=heads), :] = jnp.where(low_half, val, turned)
                head_buf[p, pl.ds(2 * pair + 1, seq, stride=heads), :] = jnp.where(
                    low_half, turned, val
                )

    def half_sum(x):
        return 0.5 * jnp.sum(x, axis=1, keepdims=True)

    recept, key, value = head_buf[0], head_buf[1], head_buf[2]
    decay = jnp.exp(-jax.nn.sigmoid(head_buf[3]) * EXP_HALF)
    rate = jax.nn.sigmoid(head_buf[4])
    unit = key * lax.rsqrt(half_sum(key * key) + KEY_EPS)
    rated = rate * recept
    removed_by = half_sum(unit * rated)
    added_by = half_sum(key * rated)
    left = (decay * recept).astype(bf16)
    right = unit.astype(bf16)
    step = 512
    left_wide = jnp.concatenate([left] * (step // 128), axis=1)
    right_wide = jnp.concatenate([right] * (step // 128), axis=1)
    read_left = jnp.zeros((rows, 128), f32)
    read_right = jnp.zeros((rows, 128), f32)
    for c in range(HEAD * HEAD // step):
        block = v_state[:, c * step : (c + 1) * step]
        ones = ones_map[c * step : (c + 1) * step, :]
        read_left += jnp.dot(block * left_wide, ones, preferred_element_type=f32)
        read_right += jnp.dot(block * right_wide, ones, preferred_element_type=f32)
    readout = read_left - read_right * removed_by + value * added_by
    centred = readout - half_sum(readout) / HEAD
    spread = half_sum(centred * centred) / HEAD
    head_buf[0] = centred * lax.rsqrt(spread + GN_EPS)
    for pair in range(heads // 2):
        even = head_buf[0, pl.ds(2 * pair, seq, stride=heads), :]
        odd = head_buf[0, pl.ds(2 * pair + 1, seq, stride=heads), :]
        span = slice(pair * 128, (pair + 1) * 128)
        mix_buf[chip, :, span] = (jnp.where(low_half, even, odd) * head_gain[:, span]).astype(bf16)

    gather_start(mix_buf, mix_send, mix_recv)
    drain(chips - 1, lambda k: prod_copy(k + 1, chip))

    @pl.when(owner != my_t)
    def _():
        prod_copy(0, chip).wait_send()

    ld_wout.wait()
    swap_late[0].wait_recv()
    gather_finish(mix_buf, mix_send, mix_recv)
    attended = jnp.dot(
        mix_buf[...].reshape(total_rows, quarter), v_wout[...], preferred_element_type=f32
    )
    token = tok_buf[:, :, pl.ds(pl.multiple_of(slot * cols, 128), cols)].astype(f32)
    attended += jnp.where(owner == my_t, token.reshape(total_rows, cols), 0.0)
    half_rows = total_rows // tp_n
    att_f[...] = attended.reshape(tp_n, half_rows, cols)
    att_out[...] = att_f[1 - my_t].astype(bf16)
    att_copy = remote(att_out, att_in, att_send, att_recv, me, 1 - my_t)
    att_copy.start()
    gather_drain(mix_buf, mix_send, mix_recv)
    att_copy.wait_recv()
    res_buf[chip, my_t] = (att_f[my_t] + att_in[...].astype(f32)).astype(bf16)

    def res_copy(i, c, e_to, t_to):
        return remote(
            res_buf.at[c, my_t], res_buf.at[c, my_t], res_send.at[i], res_recv.at[c, my_t], e_to, t_to
        )

    def res_arrived(c, t):
        remote(
            res_buf.at[c, t], res_buf.at[c, t], res_send.at[0], res_recv.at[c, t], me, my_t
        ).wait_recv()

    def res_spread(k):
        c = flip(plane, k) * 2 + side
        res_copy(planes + 3 * k, c, at(plane, 1 - side), 1 - my_t).start()
        res_copy(planes + 3 * k + 1, c, at(plane, 1 - side), my_t).start()
        res_copy(planes + 3 * k + 2, c, at(plane, side), 1 - my_t).start()

    for k in far_first:
        res_copy(k, chip, at(flip(plane, k), side), my_t).start()
    res_spread(0)
    for copy in ld_shared + ld_expert:
        copy.wait()
    for copy in swap_late[1:]:
        copy.wait_recv()
    for k in far_first:
        res_arrived(flip(plane, k) * 2 + side, my_t)
        res_spread(k)

    own_rows = pl.ds(pl.multiple_of(lax.rem(chip, group) * seq, seq), seq)
    own_half = chip // group
    square_sum = jnp.zeros((total_rows, 1), f32)
    sums = [jnp.zeros((total_rows, v_gate.shape[2]), f32) for _ in range(4)]
    own_sums = [jnp.zeros((seq, v_sgate.shape[1]), f32) for _ in range(2)]
    for x in (0, 1):
        for k in [0] + far_first:
            c = flip(plane, k) * 2 + (1 - side if x else side)
            if x:
                res_arrived(c, my_t)
            res_arrived(c, 1 - my_t)
            span = pl.ds(pl.multiple_of(c * cols, 128), cols)
            part = res_buf[c].astype(f32).reshape(total_rows, cols)
            square_sum += jnp.sum(part * part, axis=1, keepdims=True)
            gained = (part * moe_gain[:, span]).astype(bf16)
            for j in range(2):
                sums[j] += jnp.dot(gained, v_gate[j, span, :], preferred_element_type=f32)
                sums[2 + j] += jnp.dot(gained, v_up[j, span, :], preferred_element_type=f32)
            own = res_buf[c, own_half, own_rows, :].astype(f32)
            own = (own * moe_gain[:, span]).astype(bf16)
            own_sums[0] += jnp.dot(own, v_sgate[span, :], preferred_element_type=f32)
            own_sums[1] += jnp.dot(own, v_sup[span, :], preferred_element_type=f32)

    def gated(g, u):
        return g * jax.nn.sigmoid(g) * u

    factor = lax.rsqrt(square_sum / width + RMS_EPS)
    tail = tok_buf[:, :, quarter:].astype(f32).reshape(total_rows, 128)
    lanes = lax.broadcasted_iota(jnp.int32, (total_rows, 128), 1) % HEAD
    hidden = []
    for j in range(2):
        mine = jnp.sum(jnp.where(lanes == chip * 2 + j, tail, 0.0), axis=1, keepdims=True)
        hidden.append((gated(sums[j] * factor, sums[2 + j] * factor) * mine).astype(bf16))
    hidden = jnp.concatenate(hidden, axis=1)
    own_res = jnp.zeros((seq, 1), f32)
    for c in range(chips):
        part = res_buf[c, own_half, own_rows, :].astype(f32)
        own_res += jnp.sum(part * part, axis=1, keepdims=True)
    own_factor = lax.rsqrt(own_res / width + RMS_EPS)
    shared_hidden = gated(own_sums[0] * own_factor, own_sums[1] * own_factor).astype(bf16)
    down = v_down[...].reshape(2 * v_down.shape[1], width)
    for t in range(tp_n):
        span = slice(t * quarter, (t + 1) * quarter)
        routed = jnp.dot(hidden, down[:, span], preferred_element_type=f32)
        y_buf[t] = routed.astype(bf16).reshape(chips, seq, quarter)
        shared_part = jnp.dot(shared_hidden, v_sdown[:, span], preferred_element_type=f32)
        y_buf[t, chip] = (y_buf[t, chip].astype(f32) + shared_part).astype(bf16)

    turns = ((1, 1), (1, 0), (0, 1))

    def ret_copy(k, j):
        dx, dy = turns[j]
        z = flip(plane, k)
        x_to = 1 - side if dx else side
        t_to = 1 - my_t if dy else my_t
        return remote(
            y_buf.at[t_to, z * 2 + x_to],
            r_in.at[j, z],
            r_send.at[3 * k + j],
            r_recv.at[j, z],
            at(plane, x_to),
            t_to,
        )

    def sum_copy(k):
        z = flip(plane, k)
        return remote(s_buf.at[z], z_in.at[plane], s_send.at[k], s_recv.at[plane], at(z, side), my_t)

    order = far_first + [0]
    for k in order:
        for j in range(3):
            ret_copy(k, j).start()
    total = jnp.zeros((seq, quarter), f32)
    for k in order:
        z = flip(plane, k)
        total = y_buf[my_t, z * 2 + side].astype(f32)
        for j in range(3):
            ret_copy(k, j).wait_recv()
            total += r_in[j, z].astype(f32)
        if k:
            s_buf[z] = total.astype(bf16)
            sum_copy(k).start()
    for g in range(group):
        part = res_buf[my_t * group + g, own_half, own_rows, :].astype(f32)
        s_own = total[:, g * cols : (g + 1) * cols] + part
        att_f[0, pl.ds(g * seq, seq), :] = s_own
    for k in range(1, planes):
        res_copy(k, chip, me, my_t).wait_send()
    drain(3 * planes, lambda k: res_copy(planes + k, chip, me, my_t))
    att_copy.wait_send()
    for copy in swap_late:
        copy.wait_send()
    for k in order:
        for j in range(3):
            ret_copy(k, j).wait_send()
    for k in far_first:
        z = flip(plane, k)
        remote(s_buf.at[z], z_in.at[z], s_send.at[k], s_recv.at[z], me, my_t).wait_recv()
    for g in range(group):
        span = slice(g * cols, (g + 1) * cols)
        res = att_f[0, pl.ds(g * seq, seq), :]
        for k in far_first:
            res += z_in[flip(plane, k), :, span].astype(f32)
        out[:, span] = res.astype(bf16)
    for k in far_first:
        sum_copy(k).wait_send()


def fused_body(*args):
    args = list(args)
    tokens, state, w_recept = args[0], args[1], args[3]
    seq, quarter = tokens.shape
    ep_n, tp_n = lax.axis_size("ep"), lax.axis_size("tp")
    colw = w_recept.shape[1]
    width = quarter * tp_n
    heads = state.shape[1]
    chips = ep_n // 2
    group, planes, cols = chips // tp_n, chips // 2, 2 * colw
    args[1] = state.reshape(seq * heads, state.shape[2])
    for i in (2, 8, 9, 10, 12):
        args[i] = args[i].reshape(1, -1)
    for i in (13, 14):
        args[i] = args[i].T
    hidden, shared = args[15].shape[2], args[18].shape[1]
    bf16, f32, dma = jnp.bfloat16, jnp.float32, pltpu.SemaphoreType.DMA
    vmem = {2, 8, 9, 10, 12, 13, 14}
    specs = [
        pl.BlockSpec(memory_space=pltpu.VMEM if i in vmem else pl.ANY) for i in range(len(args))
    ]
    half_rows = chips * seq // tp_n
    scratch = [
        pltpu.VMEM((chips, seq, quarter + 128), bf16),
        pltpu.VMEM((tp_n, seq, 128), f32),
        pltpu.VMEM((chips, seq, 5 * cols), bf16),
        pltpu.VMEM((tp_n, group, seq, 5 * cols), bf16),
        pltpu.VMEM((chips, seq, quarter), bf16),
        pltpu.VMEM((tp_n, half_rows, cols), f32),
        pltpu.VMEM((half_rows, cols), bf16),
        pltpu.VMEM((half_rows, cols), bf16),
        pltpu.VMEM((chips, tp_n, half_rows, cols), bf16),
        pltpu.VMEM((tp_n, chips, seq, quarter), bf16),
        pltpu.VMEM((3, planes, seq, quarter), bf16),
        pltpu.VMEM((planes, seq, quarter), bf16),
        pltpu.VMEM((planes, seq, quarter), bf16),
        pltpu.VMEM((5, seq * heads, 128), f32),
        pltpu.VMEM((HEAD * HEAD, 128), bf16),
        pltpu.VMEM(args[1].shape, bf16),
        pltpu.VMEM((quarter, 5 * cols), bf16),
        pltpu.VMEM((quarter, cols), bf16),
        pltpu.VMEM((2, width, hidden), bf16),
        pltpu.VMEM((2, width, hidden), bf16),
        pltpu.VMEM((2, hidden, width), bf16),
        pltpu.VMEM((width, shared), bf16),
        pltpu.VMEM((width, shared), bf16),
        pltpu.VMEM((shared, width), bf16),
        dma((16,)),
        dma((9,)),
        dma((9,)),
        dma((2 * planes - 1,)),
        dma((chips,)),
        dma(()),
        dma(()),
        dma((chips,)),
        dma((tp_n, group)),
        dma((2 * planes - 1,)),
        dma((chips,)),
        dma(()),
        dma(()),
        dma((4 * planes,)),
        dma((chips, tp_n)),
        dma((3 * planes,)),
        dma((3, planes)),
        dma((planes,)),
        dma((planes,)),
    ]
    return pl.pallas_call(
        functools.partial(fused_kernel, (ep_n, tp_n, seq, quarter, colw, width)),
        out_shape=jax.ShapeDtypeStruct((seq, quarter), bf16),
        in_specs=specs,
        out_specs=pl.BlockSpec(memory_space=pltpu.VMEM),
        scratch_shapes=scratch,
        compiler_params=pltpu.CompilerParams(
            collective_id=0, has_side_effects=True, vmem_limit_bytes=60 * 1024 * 1024
        ),
        name="layer_step",
    )(*args)


def layer(*args):
    ep_n, tp_n = lax.axis_size("ep"), lax.axis_size("tp")
    if fits_fused(ep_n, tp_n, args[3].shape[1], args[1].shape[1], args[0].shape[1]):
        return fused_body(*args)
    return body(*args)


def solution(mesh):
    placed = (
        P("ep", "tp"),
        P("ep", "tp", None),
        P("tp"),
        P("tp", "ep"),
        P("tp", "ep"),
        P("tp", "ep"),
        P("tp", "ep"),
        P("tp", "ep"),
        P("tp"),
        P("tp"),
        P("tp"),
        P("tp", "ep"),
        P(),
        P("ep", None),
        P("ep", None),
        P("ep", None, "tp"),
        P("ep", None, "tp"),
        P("ep", "tp", None),
        P(None, "tp"),
        P(None, "tp"),
        P("tp", None),
    )
    return jax.shard_map(layer, mesh=mesh, in_specs=placed, out_specs=P("ep", "tp"), check_vma=False)
```

time: 71.1 us -> 59.6 us (0.84)
  Pallas kernels: 69.5 us -> 58 us
    pallas_call x1, Pallas kernels: 69.5 us -> 58 us  [fused_body(): pl.pallas_call(functools.partial(fused_kernel, (ep_n, tp_n, seq, quarter,...]
where the time goes in v1:
time: 59.6 us; the launch traced here: 59.4 us
  Pallas kernels  58 us (97%)
  local copies, waits for them, and re-layouts  1.38 us (2%)
    pallas_call x1, Pallas kernels, fused_body(): pl.pallas_call(functools.partial(fused_kernel, (ep_n, tp_n, seq, quarter,...  58 us
    unnamed x1, local copies, waits for them, and re-layouts  1.38 us

profile of v1, /device:TPU:0, one launch (start us, length us, event | category | flops | bytes accessed | tf_op | source)
XLA Modules:
  0.0 59.4 jit_solution(233508868326783093)
XLA Ops:
  0.0 58.0 %layer_step.1 = bf16[16,1024]{1,0:T(8,128)(2,1)} custom-call(bf16[16,1024]{1,0:T(8,128)(2,1)} %tokens.1, bf16[256,4096]{1,0:T(8,128)(2,1)} %bitcast.8, f32[1,1024]{1,0:T(1,128)} %bitcast.10, bf16[1024,128]{1,0:T(8,128)(2,1)} %w_recept.1, bf16[1024,128]{1,0:T(8,128)(2,1)} %w_key.1, bf16[1024,128]{1,0:T(8,128)(2,1)} %w_value.1, bf16[1024,128]{1,0:T(8,128)(2,1)} %w_decay.1, ...), custom_call_target="tpu_custom_call" | custom-call | tf_op jit(solution)/shard_map/layer_step/pallas_call | solution.py:731
  58.0 1.4 %copy.23 = bf16[16,1024]{1,0:T(8,128)(2,1)} copy(bf16[16,1024]{1,0:T(8,128)(2,1)} %layer_step.1) | data formatting | bytes 65536
